TPU v7x, 32 devices: a whole 2x2x4 slice. The times are simulated.
32 devices in a mesh: sp: 8 (over z, x), tp: 4 (over y, core).
Axes of the slice: x: 2, y: 2, z: 4, core: 2. Of those that a mesh axis runs over, the one named last changes fastest.
Arguments:
- residual_in: bfloat16 [4096, 2048], P('sp'), may hold values from -6 to 6
- gate_in: bfloat16 [4096, 2048], P('sp', 'tp'), may hold values from -6 to 6
- value_in: bfloat16 [4096, 2048], P('sp', 'tp'), may hold values from -6 to 6
- conv_weight: float32 [4, 2048], P(None, 'tp'), may hold values from -3 to 3
- rate_weight: bfloat16 [32, 64, 64], P('tp'), may hold values from -0.75 to 0.75
- input_weight: bfloat16 [32, 64, 64], P('tp'), may hold values from -0.75 to 0.75
- decay_base: float32 [2048], P('tp'), may hold values from 3.0517578e-06 to 0.015, as said below
- step_scale: float32 [4096, 2048], P('sp', 'tp'), may hold values from 0.25 to 57344, as said below
- out_weight: bfloat16 [2048, 2048], P('tp'), may hold values from -0.375 to 0.375
- norm_gain: float32 [2048], replicated, may hold values from 0.1 to 1.9
- up_weight: bfloat16 [2048, 8192], P('sp', 'tp'), may hold values from -0.125 to 0.125
- down_weight: bfloat16 [2048, 8192], P('sp', 'tp'), may hold values from -0.0625 to 0.0625
Outputs:
- block_out: bfloat16 [4096, 2048], P(('sp', 'tp'))
Inputs may be any that keep to these rules, and one draw needn't show every extreme that they name: `decay_base`: positive. `step_scale`: positive.
All inputs are finite; a program needn't handle non-finite values.
Results may differ from a plain program's by a relative error of at most 0.018.
Values may be sent and summed in bfloat16 or wider, within the bound.
A program may use at most 128 MiB of HBM per device.

v0:
```python
import math
import jax
import jax.numpy as jnp
from jax import lax
from jax.sharding import PartitionSpec as P


def shifted(block, axis, distance):
    devices = range(lax.axis_size(axis))
    route = [(i - distance, i) for i in devices if i - distance in devices]
    return lax.ppermute(block, axis, route)


def carried_in(part, axis, combine, identity):
    place = lax.axis_index(axis)
    gathered = jax.tree.map(lambda a: lax.all_gather(a, axis), part)
    state = jax.tree.map(lambda a, e: jnp.zeros_like(a) + jnp.asarray(e, a.dtype), part, identity)

    def one(turn, state):
        return combine(
            state, jax.tree.map(lambda a: lax.dynamic_index_in_dim(a, turn, 0, False), gathered)
        )

    return lax.fori_loop(0, place, one, state)


def chain_join(earlier, later):
    return (earlier[0] * later[0], later[0] * earlier[1] + later[1])


def rounded(term):
    return lax.optimization_barrier(term.astype(jnp.bfloat16)).astype(jnp.float32)


def settle_rows(rows_in, norm_gain):
    widened = rows_in.astype(jnp.float32)
    factor = lax.rsqrt(jnp.mean(widened * widened, axis=-1, keepdims=True) + 1e-06)
    return (widened * factor * norm_gain).astype(jnp.bfloat16)


def step_rows(carry, inputs):
    keep_row, drive_row = inputs
    new_product = carry[0] * keep_row
    new_state = keep_row * carry[1] + drive_row
    return ((new_product, new_state), (new_product, new_state))


def local(
    residual_in,
    gate_in,
    value_in,
    conv_weight,
    rate_weight,
    input_weight,
    decay_base,
    step_scale,
    out_weight,
    norm_gain,
    up_weight,
    down_weight,
):
    row_count = value_in.shape[0]
    tap_count = conv_weight.shape[0]
    channel_count = value_in.shape[1]
    earlier_rows = shifted(value_in[row_count - tap_count + 1 :], "sp", 1)
    padded = jnp.concatenate([earlier_rows, value_in], axis=0).astype(jnp.float32)
    filtered_rows = jnp.zeros(value_in.shape, jnp.float32)
    for offset in range(tap_count):
        filtered_rows = filtered_rows + padded[offset : offset + row_count] * conv_weight[offset]
    smoothed = filtered_rows.astype(jnp.bfloat16)
    grouped = smoothed.reshape(row_count, rate_weight.shape[0], rate_weight.shape[1])
    rate_gate = jax.nn.sigmoid(
        jnp.einsum("tnd,nde->tne", grouped, rate_weight, preferred_element_type=jnp.float32)
    ).reshape(row_count, -1)
    input_gate = jax.nn.sigmoid(
        jnp.einsum("tnd,nde->tne", grouped, input_weight, preferred_element_type=jnp.float32)
    ).reshape(row_count, -1)
    log_keep = -8.0 * step_scale * rate_gate * decay_base[None, :]
    drive = jnp.sqrt(-jnp.expm1(2.0 * log_keep)) * input_gate * smoothed.astype(jnp.float32)
    block_rows = math.gcd(row_count, 16)
    block_count = row_count // block_rows
    keep_blocks = (
        jnp.exp(log_keep).reshape(block_count, block_rows, channel_count).transpose(1, 0, 2)
    )
    drive_blocks = drive.reshape(block_count, block_rows, channel_count).transpose(1, 0, 2)
    start_carry = (
        jnp.ones((block_count, channel_count), jnp.float32),
        jnp.zeros((block_count, channel_count), jnp.float32),
    )
    final_carry, inner = lax.scan(step_rows, start_carry, (keep_blocks, drive_blocks))
    inner_products, inner_states = inner
    prefix_products, prefix_states = lax.associative_scan(chain_join, final_carry, axis=0)
    carried = carried_in(
        (prefix_products[-1], prefix_states[-1]),
        "sp",
        chain_join,
        (jnp.ones_like(prefix_products[-1]), jnp.zeros_like(prefix_states[-1])),
    )
    entry_products = jnp.concatenate(
        [jnp.ones((1, channel_count), jnp.float32), prefix_products[:-1]], axis=0
    )
    entry_states = jnp.concatenate(
        [jnp.zeros((1, channel_count), jnp.float32), prefix_states[:-1]], axis=0
    )
    entering = entry_states + entry_products * carried[1][None, :]
    carry_state = (
        (inner_states + inner_products * entering[None, :, :])
        .transpose(1, 0, 2)
        .reshape(row_count, channel_count)
    )
    gated = (jax.nn.gelu(gate_in.astype(jnp.float32), approximate=True) * carry_state).astype(
        jnp.bfloat16
    )
    group_rows = row_count // lax.axis_size("tp")
    own_start = lax.axis_index("tp") * group_rows
    mixed = lax.psum(
        rounded(jnp.dot(gated, out_weight, preferred_element_type=jnp.float32)).astype(
            jnp.bfloat16
        ),
        "tp",
    ).astype(jnp.float32)
    updated = (residual_in.astype(jnp.float32) + mixed).astype(jnp.bfloat16)
    normed = settle_rows(updated, norm_gain)
    own_updated = lax.dynamic_slice_in_dim(updated, own_start, group_rows, 0)
    lifted = jnp.dot(
        normed,
        lax.all_gather(up_weight, "sp", axis=0, tiled=True),
        preferred_element_type=jnp.float32,
    )
    activated = jnp.square(jax.nn.relu(lifted)).astype(jnp.bfloat16)
    partial_rows = lax.dot_general(
        activated,
        lax.all_gather(down_weight, "sp", axis=0, tiled=True),
        (((1,), (1,)), ((), ())),
        preferred_element_type=jnp.float32,
    )
    summed = lax.psum_scatter(
        rounded(partial_rows).astype(jnp.bfloat16), "tp", scatter_dimension=0, tiled=True
    ).astype(jnp.float32)
    return (own_updated.astype(jnp.float32) + summed).astype(jnp.bfloat16)


def solution(mesh):
    in_specs = (
        P("sp", None),
        P("sp", "tp"),
        P("sp", "tp"),
        P(None, "tp"),
        P("tp", None, None),
        P("tp", None, None),
        P("tp"),
        P("sp", "tp"),
        P("tp", None),
        P(),
        P("sp", "tp"),
        P("sp", "tp"),
    )
    out_specs = P(("sp", "tp"), None)
    return jax.shard_map(local, mesh=mesh, in_specs=in_specs, out_specs=out_specs, check_vma=False)
```

profile of v0, /device:TPU:0, one launch (start us, length us, event | category | flops | bytes accessed | tf_op | source)
XLA Modules:
  0.0 487.0 jit_solution(7108042623336338407)
XLA Ops:
  8.4 4.9 %collective-permute-start = (bf16[3,512]{0,1:T(8,128)(2,1)S(1)}, bf16[3,512]{0,1:T(8,128)(2,1)S(1)}, u32[]{:S(2)}, u32[]{:S(2)}) collective-permute-start(bf16[3,512]{0,1:T(8,128)(2,1)S(1)} %copy.31), channel_id=1, source_target_pairs={{0,4},{4,8},{8,12},{12,16},{16,20},{20,24},{24,28},{1,5},{5,9},{9,... | collective-permute-start | bytes 9224 | tf_op jit(solution)/shard_map/ppermute | solution.py:11
  22.1 2.7 fusion.24
  24.7 2.6 copy.34
  28.7 92.3 %while.30 = (s32[]{:T(128)}, f32[32,512]{1,0:T(8,128)S(1)}, f32[32,512]{1,0:T(8,128)S(1)}, f32[16,32,512]{2,0,1:T(8,128)}, f32[16,32,512]{2,0,1:T(8,128)}, /*ind...) while((s32[]{:T(128)}, f32[32,512]{1,0:T(8,128)S(1)}, ...), condition=%wide.region_1.2_spmd.clone, body=%wide.region_0.1_spmd.clone.sunk | while | flops 81923 | bytes 1179763 | solution.py:90
  30.1 2.1 dynamic_update_slice.12
  32.3 2.1 dynamic_update_slice.11
  35.9 2.1 dynamic_update_slice.12
  38.1 2.1 dynamic_update_slice.11
  41.7 2.1 dynamic_update_slice.12
  43.9 2.1 dynamic_update_slice.11
  47.5 2.1 dynamic_update_slice.12
  53.3 2.1 dynamic_update_slice.12
  59.1 2.1 dynamic_update_slice.12
  64.8 2.1 dynamic_update_slice.12
  70.6 2.1 dynamic_update_slice.12
  76.4 2.1 dynamic_update_slice.12
  82.2 2.1 dynamic_update_slice.12
  87.9 2.1 dynamic_update_slice.12
  93.7 2.1 dynamic_update_slice.12
  99.4 2.1 dynamic_update_slice.12
  105.2 2.1 dynamic_update_slice.12
  110.9 2.1 dynamic_update_slice.12
  116.7 2.1 dynamic_update_slice.12
  125.3 26.6 %all-gather.1 = f32[8,1,512]{2,1,0:T(1,128)S(1)} all-gather(f32[1,1,512]{2,1,0:T(1,128)S(1)} %get-tuple-element.192), channel_id=1, replica_groups=mesh['sp'=8,'tp'=4] {'sp'}, dimensions={0}, use_global_device_ids=true | all-gather | bytes 18432 | tf_op jit(solution)/shard_map/all_gather | solution.py:16
  151.9 26.1 %all-gather = f32[8,1,512]{2,1,0:T(1,128)S(1)} all-gather(f32[1,1,512]{2,1,0:T(1,128)S(1)} %get-tuple-element.193), channel_id=1, replica_groups=mesh['sp'=8,'tp'=4] {'sp'}, dimensions={0}, use_global_device_ids=true | all-gather | bytes 18432 | tf_op jit(solution)/shard_map/all_gather | solution.py:16
  180.2 2.6 convolution_convert_fusion.1
  184.2 47.5 %all-reduce.24.cloned.1.call-done = bf16[512,2048]{1,0:T(8,128)(2,1)} async-done(((bf16[512,2048]{1,0:T(8,128)(2,1)}), bf16[512,2048]{1,0:T(8,128)(2,1)}) %all-reduce.24.cloned.1.call-update) | async-done | bytes 2097168 | tf_op jit(solution)/shard_map/psum | solution.py:116
  231.8 4.6 fusion.1
  236.3 70.7 %all-gather.5.cloned.1.call-done = bf16[2048,2048]{1,0:T(8,128)(2,1)} async-done(((bf16[256,2048]{1,0:T(8,128)(2,1)}), bf16[2048,2048]{1,0:T(8,128)(2,1)}) %all-gather.5.cloned.1.call-update) | async-done | bytes 8388624 | tf_op jit(solution)/shard_map/all_gather | solution.py:127
  307.0 124.4 %all-gather.7.cloned.1.call-done = bf16[2048,2048]{1,0:T(8,128)(2,1)} async-done(((bf16[256,2048]{1,0:T(8,128)(2,1)}), bf16[2048,2048]{1,0:T(8,128)(2,1)}) %all-gather.7.cloned.1.call-update) | async-done | bytes 8388624 | tf_op jit(solution)/shard_map/all_gather | solution.py:133
  431.4 16.6 %convolution_convert_fusion = bf16[512,2048]{1,0:T(8,128)(2,1)} fusion(bf16[2048,2048]{1,0:T(8,128)(2,1)} %all-gather.7.cloned.1.call-done, bf16[2048,2048]{1,0:T(8,128)(2,1)} %all-gather.5.cloned.1.call-done, bf16[512,2048]{1,0:T(8,128)(2,1)} %get-tuple-element.157, f32[2048]{0:T(1024)S(1)} %copy-done.7, f32[512]{0:T(512)S(1)} %add_rsqrt_fusion), kind=kOutput, calls=%fused_computation.17 | convolution fusion | flops 8598323200 | bytes 20981760 | tf_op jit(solution)/shard_map/dot_general | solution.py:131
  448.0 29.5 %reduce-scatter.2.cloned.1.call-done = bf16[128,2048]{1,0:T(8,128)(2,1)} async-done(((bf16[512,2048]{1,0:T(8,128)(2,1)}), bf16[128,2048]{1,0:T(8,128)(2,1)}) %reduce-scatter.2.cloned.1.call-update) | async-done | bytes 524304 | tf_op jit(solution)/shard_map/reduce_scatter | solution.py:137
  (197 shorter events, 72.1 us)
Async XLA Ops:
  7.4 172.8 %copy-start = (bf16[512,2048]{1,0:T(8,128)(2,1)S(1)}, bf16[512,2048]{1,0:T(8,128)(2,1)}, u32[]{:S(2)}) copy-start(bf16[512,2048]{1,0:T(8,128)(2,1)} %param.24) | copy-start | bytes 6291460
  7.4 224.4 %all-reduce.24.cloned.1.call-start = ((), (), s32[]{:S(2)}) async-start(), calls=%async_computation.1 | async-start | bytes 4194304 | tf_op jit(solution)/shard_map/psum | solution.py:116
  8.4 9.4 %collective-permute-start = (bf16[3,512]{0,1:T(8,128)(2,1)S(1)}, bf16[3,512]{0,1:T(8,128)(2,1)S(1)}, u32[]{:S(2)}, u32[]{:S(2)}) collective-permute-start(bf16[3,512]{0,1:T(8,128)(2,1)S(1)} %copy.31), channel_id=1, source_target_pairs={{0,4},{4,8},{8,12},{12,16},{16,20},{20,24},{24,28},{1,5},{5,9},{9,... | collective-permute-start | bytes 9224 | tf_op jit(solution)/shard_map/ppermute | solution.py:11
  19.1 1.3 copy-start.5
  20.5 0.9 copy-start.6
  21.4 0.7 copy-start.4
  24.7 2.6 copy-start.1
  121.0 57.2 %copy-start.2 = (f32[16,32,512]{2,0,1:T(8,128)S(1)}, f32[16,32,512]{2,0,1:T(8,128)}, u32[]{:S(2)}) copy-start(f32[16,32,512]{2,0,1:T(8,128)} %get-tuple-element.90) | copy-start | bytes 3145732
  178.1 1.6 copy-start.3
  182.8 124.2 %all-gather.5.cloned.1.call-start = ((), (), s32[]{:S(2)}) async-start(), calls=%async_computation.2 | async-start | bytes 9437184 | tf_op jit(solution)/shard_map/all_gather | solution.py:127
  183.4 248.0 %all-gather.7.cloned.1.call-start = ((), (), s32[]{:S(2)}) async-start(), calls=%async_computation.3 | async-start | bytes 9437184 | tf_op jit(solution)/shard_map/all_gather | solution.py:133
  184.0 247.4 %copy-start.7 = (f32[2048]{0:T(1024)S(1)}, f32[2048]{0:T(1024)}, u32[]{:S(2)}) copy-start(f32[2048]{0:T(1024)} %param.25) | copy-start | bytes 24580
  184.0 293.4 %reduce-scatter.2.cloned.1.call-start = ((), (), s32[]{:S(2)}) async-start(), calls=%async_computation.4 | async-start | bytes 2621440 | tf_op jit(solution)/shard_map/reduce_scatter | solution.py:137
Sparse Core Ops, SparseCore 0:
  182.9 48.7 all-reduce.23
  448.1 29.3 reduce-scatter.1
Sparse Core Ops, SparseCore 1:
  185.4 121.5 all-gather.4
  309.0 122.3 all-gather.6
where the time goes:
time: 489 us; the launch traced here: 487 us
  waiting for transfers between devices  273 us (56%)
  local copies, waits for them, and re-layouts  104 us (21%)
  blocking collectives  52.7 us (11%)
  matrix products  20.2 us (4%)
  other arithmetic  15.8 us (3%)
  between operations  15.3 us (3%)
  starting transfers between devices  5.19 us (1%)
    all_gather x1, waiting for transfers between devices, local(): lax.all_gather(down_weight, 'sp', axis=0, tiled=True)  124 us
    all_gather x1, waiting for transfers between devices, local(): lax.all_gather(up_weight, 'sp', axis=0, tiled=True)  70.7 us
    dynamic_update_slice x64, local copies, waits for them, and re-layouts, local(): lax.scan(step_rows, start_carry, (keep_blocks, drive_blocks))  70.1 us
    all_gather x2, blocking collectives, carried_in(): gathered = jax.tree.map(lambda a: lax.all_gather(a, axis), part)  52.7 us
    psum x1, waiting for transfers between devices, local(): lax.psum(rounded(jnp.dot(gated, out_weight, preferred_element_type=jnp.fl...  47.5 us
    reduce_scatter x1, waiting for transfers between devices, local(): lax.psum_scatter(rounded(partial_rows).astype(jnp.bfloat16), 'tp', scatte...  29.5 us
    dynamic_slice x16, local copies, waits for them, and re-layouts, local(): lax.scan(step_rows, start_carry, (keep_blocks, drive_blocks))  21 us
    dot_general x1, matrix products, local(): lax.dot_general(activated, lax.all_gather(down_weight, 'sp', axis=0, tile...  16.6 us
  transfers between devices with their start and end apart: 5, of which 4 were waited for; matrix products, arithmetic and copies ran while one was open for 2% of the time, Pallas kernels for 0%

commit v1 on v0

--- a/solution.py
+++ b/solution.py
@@ -113,11 +113,14 @@
     )
     group_rows = row_count // lax.axis_size("tp")
     own_start = lax.axis_index("tp") * group_rows
-    mixed = lax.psum(
-        rounded(jnp.dot(gated, out_weight, preferred_element_type=jnp.float32)).astype(
-            jnp.bfloat16
+    mixed = jnp.sum(
+        lax.all_gather(
+            rounded(jnp.dot(gated, out_weight, preferred_element_type=jnp.float32)).astype(
+                jnp.bfloat16
+            ),
+            "tp",
         ),
-        "tp",
+        axis=0,
     ).astype(jnp.float32)
     updated = (residual_in.astype(jnp.float32) + mixed).astype(jnp.bfloat16)
     normed = settle_rows(updated, norm_gain)

time: 489 us -> 546 us (1.12)
  waiting for transfers between devices: 273 us -> 324 us
  other arithmetic: 15.8 us -> 23.2 us
    all_gather x0 -> x1, waiting for transfers between devices: none -> 54.1 us  [local(): lax.all_gather(rounded(jnp.dot(gated, out_weight, preferred_element_type=...]
    psum x1 -> x0, waiting for transfers between devices: 47.5 us -> none  [local(): lax.psum(rounded(jnp.dot(gated, out_weight, preferred_element_type=jnp.fl...]
    all_gather x1, waiting for transfers between devices: 70.7 us -> 115 us  [local(): lax.all_gather(up_weight, 'sp', axis=0, tiled=True)]
    reduce_sum x0 -> x1, other arithmetic: none -> 7.25 us  [local(): jnp.sum(lax.all_gather(rounded(jnp.dot(gated, out_weight, preferred_eleme...]
  transfers between devices with their start and end apart: 5 -> 5, of which waited for: 4 -> 4; matrix products, arithmetic and copies ran while one was open for 2% -> 3% of each run, Pallas kernels for 0% -> 0%
where the time goes in v1:
time: 546 us; the launch traced here: 544 us
  waiting for transfers between devices  324 us (59%)
  local copies, waits for them, and re-layouts  104 us (19%)
  blocking collectives  52.7 us (10%)
  other arithmetic  23.2 us (4%)
  matrix products  20.2 us (4%)
  between operations  13.6 us (2%)
    all_gather x1, waiting for transfers between devices, local(): lax.all_gather(down_weight, 'sp', axis=0, tiled=True)  125 us
    all_gather x1, waiting for transfers between devices, local(): lax.all_gather(up_weight, 'sp', axis=0, tiled=True)  115 us
    dynamic_update_slice x64, local copies, waits for them, and re-layouts, local(): lax.scan(step_rows, start_carry, (keep_blocks, drive_blocks))  70.1 us
    all_gather x1, waiting for transfers between devices, local(): lax.all_gather(rounded(jnp.dot(gated, out_weight, preferred_element_type=...  54.1 us
    all_gather x2, blocking collectives, carried_in(): gathered = jax.tree.map(lambda a: lax.all_gather(a, axis), part)  52.7 us
    reduce_scatter x1, waiting for transfers between devices, local(): lax.psum_scatter(rounded(partial_rows).astype(jnp.bfloat16), 'tp', scatte...  29.5 us
    dynamic_slice x16, local copies, waits for them, and re-layouts, local(): lax.scan(step_rows, start_carry, (keep_blocks, drive_blocks))  21 us
    dot_general x1, matrix products, local(): lax.dot_general(activated, lax.all_gather(down_weight, 'sp', axis=0, tile...  16.6 us
  transfers between devices with their start and end apart: 5, of which 4 were waited for; matrix products, arithmetic and copies ran while one was open for 3% of the time, Pallas kernels for 0%

profile of v1, /device:TPU:0, one launch (start us, length us, event | category | flops | bytes accessed | tf_op | source)
XLA Modules:
  0.0 544.0 jit_solution(8757164343814488147)
XLA Ops:
  7.6 4.9 collective-permute-start
  21.2 2.7 fusion.24
  23.9 2.6 copy.34
  27.8 92.3 %while.30 = (s32[]{:T(128)}, f32[32,512]{1,0:T(8,128)S(1)}, f32[32,512]{1,0:T(8,128)S(1)}, f32[16,32,512]{2,0,1:T(8,128)}, f32[16,32,512]{2,0,1:T(8,128)}, /*ind...) while((s32[]{:T(128)}, f32[32,512]{1,0:T(8,128)S(1)}, ...), condition=%wide.region_1.2_spmd.clone, body=%wide.region_0.1_spmd.clone.sunk | while | flops 81923 | bytes 1179763 | solution.py:90
  29.3 2.1 dynamic_update_slice.12
  31.5 2.1 dynamic_update_slice.11
  35.1 2.1 dynamic_update_slice.12
  37.3 2.1 dynamic_update_slice.11
  40.9 2.1 dynamic_update_slice.12
  46.7 2.1 dynamic_update_slice.12
  52.4 2.1 dynamic_update_slice.12
  58.2 2.1 dynamic_update_slice.12
  64.0 2.1 dynamic_update_slice.12
  69.8 2.1 dynamic_update_slice.12
  75.6 2.1 dynamic_update_slice.12
  81.3 2.1 dynamic_update_slice.12
  87.1 2.1 dynamic_update_slice.12
  92.8 2.1 dynamic_update_slice.12
  98.6 2.1 dynamic_update_slice.12
  104.3 2.1 dynamic_update_slice.12
  110.1 2.1 dynamic_update_slice.12
  115.8 2.1 dynamic_update_slice.12
  124.5 26.6 %all-gather.2 = f32[8,1,512]{2,1,0:T(1,128)S(1)} all-gather(f32[1,1,512]{2,1,0:T(1,128)S(1)} %get-tuple-element.192), channel_id=1, replica_groups=mesh['sp'=8,'tp'=4] {'sp'}, dimensions={0}, use_global_device_ids=true | all-gather | bytes 18432 | tf_op jit(solution)/shard_map/all_gather | solution.py:16
  151.1 26.1 %all-gather.1 = f32[8,1,512]{2,1,0:T(1,128)S(1)} all-gather(f32[1,1,512]{2,1,0:T(1,128)S(1)} %get-tuple-element.193), channel_id=1, replica_groups=mesh['sp'=8,'tp'=4] {'sp'}, dimensions={0}, use_global_device_ids=true | all-gather | bytes 18432 | tf_op jit(solution)/shard_map/all_gather | solution.py:16
  179.3 2.6 convolution_convert_fusion.1
  183.7 54.1 %all-gather.11.cloned.1.call-done = bf16[2048,2048]{1,0:T(8,128)(2,1)} async-done(((bf16[512,2048]{1,0:T(8,128)(2,1)}), bf16[2048,2048]{1,0:T(8,128)(2,1)}) %all-gather.11.cloned.1.call-update) | async-done | bytes 8388624 | tf_op jit(solution)/shard_map/all_gather | solution.py:117
  237.8 7.3 %reduce_sum.21 = bf16[512,2048]{1,0:T(8,128)(2,1)} reduce(bf16[4,512,2048]{2,1,0:T(8,128)(2,1)} %bitcast.83, bf16[]{:T(256)} %constant.64.clone.1), dimensions={0}, to_apply=%region_4.5 | reduce | flops 3145728 | bytes 10485762 | tf_op jit(solution)/shard_map/reduce_sum | solution.py:116
  245.1 4.7 fusion.1
  249.8 114.6 %all-gather.7.cloned.1.call-done = bf16[2048,2048]{1,0:T(8,128)(2,1)} async-done(((bf16[256,2048]{1,0:T(8,128)(2,1)}), bf16[2048,2048]{1,0:T(8,128)(2,1)}) %all-gather.7.cloned.1.call-update) | async-done | bytes 8388624 | tf_op jit(solution)/shard_map/all_gather | solution.py:130
  364.4 124.8 %all-gather.9.cloned.1.call-done = bf16[2048,2048]{1,0:T(8,128)(2,1)} async-done(((bf16[256,2048]{1,0:T(8,128)(2,1)}), bf16[2048,2048]{1,0:T(8,128)(2,1)}) %all-gather.9.cloned.1.call-update) | async-done | bytes 8388624 | tf_op jit(solution)/shard_map/all_gather | solution.py:136
  489.3 16.6 %convolution_convert_fusion = bf16[512,2048]{1,0:T(8,128)(2,1)} fusion(bf16[2048,2048]{1,0:T(8,128)(2,1)} %all-gather.9.cloned.1.call-done, bf16[2048,2048]{1,0:T(8,128)(2,1)} %all-gather.7.cloned.1.call-done, bf16[512,2048]{1,0:T(8,128)(2,1)} %get-tuple-element.157, f32[2048]{0:T(1024)S(1)} %copy-done.7, f32[512]{0:T(512)S(1)} %add_rsqrt_fusion), kind=kOutput, calls=%fused_computation.17 | convolution fusion | flops 8598323200 | bytes 20981760 | tf_op jit(solution)/shard_map/dot_general | solution.py:134
  505.9 29.5 %reduce-scatter.2.cloned.1.call-done = bf16[128,2048]{1,0:T(8,128)(2,1)} async-done(((bf16[512,2048]{1,0:T(8,128)(2,1)}), bf16[128,2048]{1,0:T(8,128)(2,1)}) %reduce-scatter.2.cloned.1.call-update) | async-done | bytes 524304 | tf_op jit(solution)/shard_map/reduce_scatter | solution.py:140
  (198 shorter events, 74.6 us)
Async XLA Ops:
  6.5 172.8 %copy-start = (bf16[512,2048]{1,0:T(8,128)(2,1)S(1)}, bf16[512,2048]{1,0:T(8,128)(2,1)}, u32[]{:S(2)}) copy-start(bf16[512,2048]{1,0:T(8,128)(2,1)} %param.24) | copy-start | bytes 6291460
  6.5 231.3 %all-gather.11.cloned.1.call-start = ((), (), s32[]{:S(2)}) async-start(), calls=%async_computation.4 | async-start | bytes 10485760 | tf_op jit(solution)/shard_map/all_gather | solution.py:117
  7.6 9.4 %collective-permute-start = (bf16[3,512]{0,1:T(8,128)(2,1)S(1)}, bf16[3,512]{0,1:T(8,128)(2,1)S(1)}, u32[]{:S(2)}, u32[]{:S(2)}) collective-permute-start(bf16[3,512]{0,1:T(8,128)(2,1)S(1)} %copy.31), channel_id=1, source_target_pairs={{0,4},{4,8},{8,12},{12,16},{16,20},{20,24},{24,28},{1,5},{5,9},{9,... | collective-permute-start | bytes 9224 | tf_op jit(solution)/shard_map/ppermute | solution.py:11
  18.3 1.3 copy-start.5
  19.6 0.9 copy-start.6
  20.5 0.7 copy-start.4
  23.9 2.6 copy-start.1
  120.1 57.2 %copy-start.2 = (f32[16,32,512]{2,0,1:T(8,128)S(1)}, f32[16,32,512]{2,0,1:T(8,128)}, u32[]{:S(2)}) copy-start(f32[16,32,512]{2,0,1:T(8,128)} %get-tuple-element.90) | copy-start | bytes 3145732
  177.3 1.6 copy-start.3
  182.0 182.4 %all-gather.7.cloned.1.call-start = ((), (), s32[]{:S(2)}) async-start(), calls=%async_computation.1 | async-start | bytes 9437184 | tf_op jit(solution)/shard_map/all_gather | solution.py:130
  182.8 306.5 %all-gather.9.cloned.1.call-start = ((), (), s32[]{:S(2)}) async-start(), calls=%async_computation.2 | async-start | bytes 9437184 | tf_op jit(solution)/shard_map/all_gather | solution.py:136
  183.5 351.9 %reduce-scatter.2.cloned.1.call-start = ((), (), s32[]{:S(2)}) async-start(), calls=%async_computation.3 | async-start | bytes 2621440 | tf_op jit(solution)/shard_map/reduce_scatter | solution.py:140
  245.1 244.2 %copy-start.7 = (f32[2048]{0:T(1024)S(1)}, f32[2048]{0:T(1024)}, u32[]{:S(2)}) copy-start(f32[2048]{0:T(1024)} %param.25) | copy-start | bytes 24580
Sparse Core Ops, SparseCore 0:
  182.1 55.6 all-gather.10
  239.9 124.4 all-gather.6
  366.6 122.6 all-gather.8
  506.0 29.3 reduce-scatter.1
